TPU v7x, 32 devices: a whole 2x2x4 slice. The times are simulated.
32 devices in a mesh: fs: 8 (over z, y), tp: 4 (over x, core).
Axes of the slice: x: 2, y: 2, z: 4, core: 2. Of those that a mesh axis runs over, the one named last changes fastest.
Arguments:
- stream: bfloat16 [3072, 2048], P('fs', 'tp'), may hold values from -3 to 3
- gain_first: float32 [2048], replicated, may hold values from 0.1 to 1.9
- gain_mixer: float32 [2048], replicated, may hold values from 0.1 to 1.9
- gain_second: float32 [2048], replicated, may hold values from 0.1 to 1.9
- gate_weight: float32 [2048, 5632], P('fs', 'tp'), may hold values from -0.125 to 0.125
- gate_scale: float32 [5632], P('tp'), may hold values from 0.5 to 2
- up_weight: float32 [2048, 5632], P('fs', 'tp'), may hold values from -0.125 to 0.125
- up_scale: float32 [5632], P('tp'), may hold values from 0.5 to 2
- down_weight: float32 [5632, 2048], P('tp', 'fs'), may hold values from -0.109375 to 0.109375
- down_scale: float32 [2048], P('tp'), may hold values from 0.5 to 2
- pool_in_weight: float32 [2048, 512], P('fs', 'tp'), may hold values from -0.125 to 0.125
- pool_in_scale: float32 [512], P('tp'), may hold values from 0.5 to 2
- pool_out_weight: float32 [512, 2048], P('tp', 'fs'), may hold values from -0.375 to 0.375
- pool_out_scale: float32 [2048], P('tp'), may hold values from 0.5 to 2
Outputs:
- layer_out: bfloat16 [3072, 2048], P('fs', 'tp')
All inputs are finite; a program needn't handle non-finite values.
Results may differ from a plain program's by a relative error of at most 0.025.
Values may be sent and summed in bfloat16 or wider, within the bound.
A program may use at most 64 MiB of HBM per device.

v0:
```python
import jax
import jax.numpy as jnp
from jax import lax
from jax.sharding import PartitionSpec as P

SEQ = 128
eps = 1e-06
WINDOWS = (2, 4, 8, 16)


def normed(own_columns, norm_gain):
    gathered = lax.all_gather(own_columns, "tp", axis=1, tiled=True)
    floats = gathered.astype(jnp.float32)
    scaled = floats * lax.rsqrt(jnp.mean(floats * floats, axis=-1, keepdims=True) + eps)
    return (scaled * norm_gain).astype(jnp.bfloat16)


def residual_add(own_columns, partial_value, column_scale, factor):
    summed = lax.psum_scatter(
        partial_value.astype(jnp.bfloat16), "tp", scatter_dimension=1, tiled=True
    ).astype(jnp.float32)
    return (own_columns.astype(jnp.float32) + factor * (summed * column_scale)).astype(jnp.bfloat16)


def pooling(pool_input):
    channels = pool_input.shape[1]
    floats = pool_input.astype(jnp.float32).reshape(-1, SEQ, channels)
    csum = jnp.concatenate(
        [jnp.zeros((floats.shape[0], 1, channels), jnp.float32), jnp.cumsum(floats, axis=1)], axis=1
    )
    position = jnp.arange(SEQ)
    channel_index = lax.axis_index("tp") * channels + jnp.arange(channels, dtype=jnp.int32)
    channel_group = channel_index * 4 // (channels * lax.axis_size("tp"))
    pooled = -floats
    for group_index, window in enumerate(WINDOWS):
        before = window // 2
        after_span = window - before
        upper_sum = jnp.pad(csum, ((0, 0), (0, after_span), (0, 0)), mode="edge")[
            :, after_span : after_span + SEQ
        ]
        lower_sum = jnp.pad(csum, ((0, 0), (before, 0), (0, 0)), mode="edge")[:, :SEQ]
        counts = (
            jnp.minimum(position + after_span, SEQ) - jnp.maximum(position - before, 0)
        ).astype(jnp.float32)
        window_mean = (upper_sum - lower_sum) / counts[None, :, None]
        select = (channel_group == group_index).astype(jnp.float32)
        pooled = pooled + window_mean * select
    return pooled.reshape(-1, channels).astype(jnp.bfloat16)


def body(
    stream,
    gain_first,
    gain_mixer,
    gain_second,
    gate_weight,
    gate_scale,
    up_weight,
    up_scale,
    down_weight,
    down_scale,
    pool_in_weight,
    pool_in_scale,
    pool_out_weight,
    pool_out_scale,
):
    gate_half = gate_weight.astype(jnp.bfloat16)
    up_half = up_weight.astype(jnp.bfloat16)
    down_half = down_weight.astype(jnp.bfloat16)
    in_half = pool_in_weight.astype(jnp.bfloat16)
    out_half = pool_out_weight.astype(jnp.bfloat16)
    in_whole, out_whole = (
        lax.all_gather(in_half, "fs", axis=0, tiled=True),
        lax.all_gather(out_half, "fs", axis=1, tiled=True),
    )
    gate_whole, up_whole, down_whole = (
        lax.all_gather(gate_half, "fs", axis=0, tiled=True),
        lax.all_gather(up_half, "fs", axis=0, tiled=True),
        lax.all_gather(down_half, "fs", axis=1, tiled=True),
    )

    def feed_forward(normed_rows):
        gate_sum = jnp.dot(normed_rows, gate_whole, preferred_element_type=jnp.float32) * gate_scale
        up_sum = jnp.dot(normed_rows, up_whole, preferred_element_type=jnp.float32) * up_scale
        hidden = (jax.nn.silu(gate_sum) * up_sum).astype(jnp.bfloat16)
        return jnp.dot(hidden, down_whole, preferred_element_type=jnp.float32)

    after_first = residual_add(stream, feed_forward(normed(stream, gain_first)), down_scale, 0.5)
    mixer_normed = normed(after_first, gain_mixer)
    pool_input = (
        jnp.dot(mixer_normed, in_whole, preferred_element_type=jnp.float32) * pool_in_scale
    ).astype(jnp.bfloat16)
    pooled = pooling(pool_input)
    tp_count = lax.axis_size("tp")
    all_pooled = lax.all_gather(pooled, "tp", axis=1, tiled=True)
    out_columns = lax.all_to_all(out_whole, "tp", split_axis=1, concat_axis=0, tiled=True)
    block_width = out_columns.shape[0] // tp_count
    pooled_blocks = all_pooled.reshape(all_pooled.shape[0], tp_count, block_width)
    weight_blocks = out_columns.reshape(tp_count, block_width, out_columns.shape[1])
    partials = jnp.einsum(
        "rbc,bcd->brd", pooled_blocks, weight_blocks, preferred_element_type=jnp.float32
    ).astype(jnp.bfloat16)
    mixed = jnp.sum(partials.astype(jnp.float32), axis=0)
    after_mix = (after_first.astype(jnp.float32) + mixed * pool_out_scale).astype(jnp.bfloat16)
    return residual_add(after_mix, feed_forward(normed(after_mix, gain_second)), down_scale, 0.5)


def solution(mesh):
    placed = (
        P("fs", "tp"),
        P(),
        P(),
        P(),
        P("fs", "tp"),
        P("tp"),
        P("fs", "tp"),
        P("tp"),
        P("tp", "fs"),
        P("tp"),
        P("fs", "tp"),
        P("tp"),
        P("tp", "fs"),
        P("tp"),
    )
    return jax.shard_map(body, mesh=mesh, in_specs=placed, out_specs=P("fs", "tp"), check_vma=False)
```

profile of v0, /device:TPU:0, one launch (start us, length us, event | category | flops | bytes accessed | tf_op | source)
XLA Modules:
  0.0 509.7 jit_solution(2998391872795220859)
XLA Ops:
  6.5 0.0 all-gather.7.cloned.1.call-start
  6.5 0.7 all-gather.7.cloned.1.call-update
  7.3 0.0 all-gather.9.cloned.1.call-start
  7.3 2.3 convert_element_type.144
  9.6 0.0 all-gather.9.cloned.1.call-update
  9.6 0.0 all-gather.11.cloned.1.call-start
  9.7 0.0 copy-done.5
  9.7 1.0 convert_element_type.145
  10.7 0.0 all-gather.11.cloned.1.call-update
  10.7 0.0 copy-start.11
  10.7 0.0 copy-start.13
  10.7 0.0 all-gather.13.cloned.1.call-start
  10.8 0.5 copy-done.6
  11.2 1.0 convert_element_type.147
  12.2 0.0 all-gather.13.cloned.1.call-update
  12.2 0.0 reduce-scatter.3.cloned.1.call-start
  12.3 19.0 %all-gather.7.cloned.1.call-done = bf16[384,2048]{1,0:T(8,128)(2,1)} async-done(((bf16[384,512]{1,0:T(8,128)(2,1)}), bf16[384,2048]{1,0:T(8,128)(2,1)}) %all-gather.7.cloned.1.call-update) | async-done | bytes 1572880 | tf_op jit(solution)/shard_map/all_gather | solution.py:12
  31.3 1.8 fusion
  33.1 0.0 copy-start.14
  33.1 92.7 %all-gather.9.cloned.1.call-done = bf16[2048,1408]{1,0:T(8,128)(2,1)} async-done(((bf16[256,1408]{1,0:T(8,128)(2,1)}), bf16[2048,1408]{1,0:T(8,128)(2,1)}) %all-gather.9.cloned.1.call-update) | async-done | bytes 5767184 | tf_op jit(solution)/shard_map/all_gather | solution.py:77
  125.8 0.0 copy-done.11
  125.8 0.0 copy-done.13
  125.8 7.1 %convolution_multiply_fusion.3 = f32[384,1408]{1,0:T(8,128)} fusion(bf16[2048,1408]{1,0:T(8,128)(2,1)} %all-gather.9.cloned.1.call-done, f32[1408]{0:T(1024)S(1)} %copy-done.13, bf16[384,2048]{1,0:T(8,128)(2,1)} %all-gather.7.cloned.1.call-done, f32[2048]{0:T(1024)S(1)} %copy-done.11, f32[384]{0:T(512)S(1)} %add_rsqrt_fusion.2), kind=kOutput, calls=%fused_computation.21 | convolution fusion | flops 2218278912 | bytes 9518080 | tf_op jit(solution)/shard_map/dot_general | solution.py:83
  133.0 85.6 %all-gather.11.cloned.1.call-done = bf16[2048,1408]{1,0:T(8,128)(2,1)} async-done(((bf16[256,1408]{1,0:T(8,128)(2,1)}), bf16[2048,1408]{1,0:T(8,128)(2,1)}) %all-gather.11.cloned.1.call-update) | async-done | bytes 5767184 | tf_op jit(solution)/shard_map/all_gather | solution.py:78
  218.5 93.2 %all-gather.13.cloned.1.call-done = bf16[1408,2048]{1,0:T(8,128)(2,1)} async-done(((bf16[1408,256]{1,0:T(8,128)(2,1)}), bf16[1408,2048]{1,0:T(8,128)(2,1)}) %all-gather.13.cloned.1.call-update) | async-done | bytes 5767184 | tf_op jit(solution)/shard_map/all_gather | solution.py:79
  311.8 0.0 copy-done.2
  311.8 0.0 copy-done.14
  311.8 11.2 %convolution_convert_fusion.1 = bf16[384,2048]{1,0:T(8,128)(2,1)} fusion(bf16[1408,2048]{1,0:T(8,128)(2,1)} %all-gather.13.cloned.1.call-done, bf16[2048,1408]{1,0:T(8,128)(2,1)} %all-gather.11.cloned.1.call-done, f32[384,1408]{1,0:T(8,128)} %convolution_multiply_fusion.3, f32[1408]{0:T(1024)S(1)} %copy-done.14, bf16[384,2048]{1,0:T(8,128)(2,1)S(1)} %copy-done.2, ...), kind=kOutput, calls=%fused_computation.23 | convolution fusion | flops 4436901888 | bytes 16858112 | tf_op jit(solution)/shard_map/dot_general | solution.py:86
  323.0 0.0 reduce-scatter.3.cloned.1.call-update
  323.0 0.0 copy-start.8
  323.0 0.0 all-gather.15.cloned.1.call-start
  323.1 26.3 %reduce-scatter.3.cloned.1.call-done = bf16[384,512]{1,0:T(8,128)(2,1)} async-done(((bf16[384,2048]{1,0:T(8,128)(2,1)}), bf16[384,512]{1,0:T(8,128)(2,1)}) %reduce-scatter.3.cloned.1.call-update) | async-done | bytes 393232 | tf_op jit(solution)/shard_map/reduce_scatter | solution.py:19
  349.3 0.0 copy-done.4
  349.3 1.9 add_convert_fusion.2
  351.2 0.0 all-gather.15.cloned.1.call-update
  351.3 0.1 copy.16
  351.4 31.7 %all_gather.34 = bf16[128,2048]{0,1:T(8,128)(2,1)S(1)} all-gather(bf16[128,256]{0,1:T(8,128)(2,1)S(1)} %copy.16), channel_id=1, replica_groups=mesh['fs'=8,'tp'=4] {'fs'}, dimensions={1}, use_global_device_ids=true | all-gather | bytes 589824 | tf_op jit(solution)/shard_map/all_gather | solution.py:74
  383.1 1.0 copy.17
  384.1 3.5 all-to-all-start
  387.6 0.0 all-gather.17.cloned.1.call-start
  387.8 31.5 %all_gather.32 = bf16[2048,128]{1,0:T(8,128)(2,1)S(1)} all-gather(bf16[256,128]{1,0:T(8,128)(2,1)S(1)} %convert_element_type.154), channel_id=1, replica_groups=mesh['fs'=8,'tp'=4] {'fs'}, dimensions={0}, use_global_device_ids=true | all-gather | bytes 589824 | tf_op jit(solution)/shard_map/all_gather | solution.py:73
  419.3 1.8 fusion.3
  421.1 0.0 copy-done.12
  421.1 2.0 fusion.20
  423.2 0.0 copy-start
  423.2 0.0 copy-start.10
  423.2 0.2 reduce_window_sum.11
  423.5 0.3 fusion.46
  423.8 0.1 copy.15
  423.9 6.7 %all_gather.33 = bf16[384,512]{0,1:T(8,128)(2,1)S(1)} all-gather(bf16[384,128]{0,1:T(8,128)(2,1)S(1)} %copy.15), channel_id=1, replica_groups=mesh['fs'=8,'tp'=4] {'tp'}, dimensions={1}, use_global_device_ids=true | all-gather | bytes 491520 | tf_op jit(solution)/shard_map/all_gather | solution.py:95
  430.6 0.0 all-to-all-done
  430.6 0.6 convert_reduce_fusion
  431.2 0.0 copy-start.15
  431.2 0.9 add_convert_fusion.1
  432.1 0.0 all-gather.17.cloned.1.call-update
  432.1 0.2 reduce-scatter.5.cloned.1.call-start
  432.4 20.1 %all-gather.17.cloned.1.call-done = bf16[384,2048]{1,0:T(8,128)(2,1)} async-done(((bf16[384,512]{1,0:T(8,128)(2,1)}), bf16[384,2048]{1,0:T(8,128)(2,1)}) %all-gather.17.cloned.1.call-update) | async-done | bytes 1572880 | tf_op jit(solution)/shard_map/all_gather | solution.py:12
  452.4 1.8 fusion.6
  454.3 7.2 %convolution_multiply_fusion.1 = f32[384,1408]{1,0:T(8,128)} fusion(bf16[2048,1408]{1,0:T(8,128)(2,1)} %all-gather.9.cloned.1.call-done, f32[1408]{0:T(1024)S(1)} %copy-done.13, bf16[384,2048]{1,0:T(8,128)(2,1)} %all-gather.17.cloned.1.call-done, f32[2048]{0:T(1024)S(1)} %copy-done.15, f32[384]{0:T(512)S(1)} %add_rsqrt_fusion), kind=kOutput, calls=%fused_computation.18 | convolution fusion | flops 2218278912 | bytes 9518080 | tf_op jit(solution)/shard_map/dot_general | solution.py:83
  461.5 11.3 %convolution_convert_fusion = bf16[384,2048]{1,0:T(8,128)(2,1)} fusion(bf16[1408,2048]{1,0:T(8,128)(2,1)} %all-gather.13.cloned.1.call-done, bf16[2048,1408]{1,0:T(8,128)(2,1)} %all-gather.11.cloned.1.call-done, f32[384,1408]{1,0:T(8,128)} %convolution_multiply_fusion.1, f32[1408]{0:T(1024)S(1)} %copy-done.14, bf16[384,2048]{1,0:T(8,128)(2,1)S(1)} %copy-done.3, ...), kind=kOutput, calls=%fused_computation.22 | convolution fusion | flops 4436901888 | bytes 16858112 | tf_op jit(solution)/shard_map/dot_general | solution.py:86
  472.8 0.0 reduce-scatter.5.cloned.1.call-update
  472.8 28.1 %reduce-scatter.5.cloned.1.call-done = bf16[384,512]{1,0:T(8,128)(2,1)} async-done(((bf16[384,2048]{1,0:T(8,128)(2,1)}), bf16[384,512]{1,0:T(8,128)(2,1)}) %reduce-scatter.5.cloned.1.call-update) | async-done | bytes 393232 | tf_op jit(solution)/shard_map/reduce_scatter | solution.py:19
  501.0 0.0 copy-done.1
  501.0 1.9 add_convert_fusion
  (38 shorter events, 0.2 us)
Async XLA Ops:
  6.5 3.2 copy-start.5
  6.5 24.7 %all-gather.7.cloned.1.call-start = ((), (), s32[]{:S(2)}) async-start(), calls=%async_computation.3 | async-start | bytes 1966080 | tf_op jit(solution)/shard_map/all_gather | solution.py:12
  7.3 118.5 %all-gather.9.cloned.1.call-start = ((), (), s32[]{:S(2)}) async-start(), calls=%async_computation.4 | async-start | bytes 6488064 | tf_op jit(solution)/shard_map/all_gather | solution.py:77
  9.6 1.6 copy-start.6
  9.6 208.9 %all-gather.11.cloned.1.call-start = ((), (), s32[]{:S(2)}) async-start(), calls=%async_computation.5 | async-start | bytes 6488064 | tf_op jit(solution)/shard_map/all_gather | solution.py:78
  10.7 115.1 %copy-start.11 = (f32[2048]{0:T(1024)S(1)}, f32[2048]{0:T(1024)}, u32[]{:S(2)}) copy-start(f32[2048]{0:T(1024)} %param.15) | copy-start | bytes 24580
  10.7 115.1 %copy-start.13 = (f32[1408]{0:T(1024)S(1)}, f32[1408]{0:T(1024)}, u32[]{:S(2)}) copy-start(f32[1408]{0:T(1024)} %param.19) | copy-start | bytes 16900
  10.7 301.1 %all-gather.13.cloned.1.call-start = ((), (), s32[]{:S(2)}) async-start(), calls=%async_computation.6 | async-start | bytes 6488064 | tf_op jit(solution)/shard_map/all_gather | solution.py:79
  12.2 337.1 %reduce-scatter.3.cloned.1.call-start = ((), (), s32[]{:S(2)}) async-start(), calls=%async_computation.7 | async-start | bytes 1966080 | tf_op jit(solution)/shard_map/reduce_scatter | solution.py:19
  33.1 278.7 %copy-start.2 = (bf16[384,2048]{1,0:T(8,128)(2,1)S(1)}, bf16[384,2048]{1,0:T(8,128)(2,1)}, u32[]{:S(2)}) copy-start(bf16[384,2048]{1,0:T(8,128)(2,1)} %all-gather.7.cloned.1.call-done) | copy-start | bytes 4718596
  33.1 278.7 %copy-start.14 = (f32[1408]{0:T(1024)S(1)}, f32[1408]{0:T(1024)}, u32[]{:S(2)}) copy-start(f32[1408]{0:T(1024)} %param.21) | copy-start | bytes 16900
  133.0 216.4 %copy-start.4 = (bf16[384,512]{1,0:T(8,128)(2,1)S(1)}, bf16[384,512]{1,0:T(8,128)(2,1)}, u32[]{:S(2)}) copy-start(bf16[384,512]{1,0:T(8,128)(2,1)} %param.14) | copy-start | bytes 1179652
  133.0 216.4 %copy-start.9 = (f32[512]{0:T(512)S(1)}, f32[512]{0:T(512)}, u32[]{:S(2)}) copy-start(f32[512]{0:T(512)} %param.23) | copy-start | bytes 6148
  323.0 28.3 %copy-start.7 = (f32[128,256]{1,0:T(8,128)S(1)}, f32[128,256]{1,0:T(8,128)}, u32[]{:S(2)}) copy-start(f32[128,256]{1,0:T(8,128)} %param.26) | copy-start | bytes 393220
  323.0 64.6 %copy-start.8 = (f32[256,128]{1,0:T(8,128)S(1)}, f32[256,128]{1,0:T(8,128)}, u32[]{:S(2)}) copy-start(f32[256,128]{1,0:T(8,128)} %param.24) | copy-start | bytes 393220
  323.0 96.3 %all-gather.15.cloned.1.call-start = ((), (), s32[]{:S(2)}) async-start(), calls=%async_computation.8 | async-start | bytes 1966080 | tf_op jit(solution)/shard_map/all_gather | solution.py:12
  383.1 38.0 %copy-start.12 = (f32[2048]{0:T(1024)S(1)}, f32[2048]{0:T(1024)}, u32[]{:S(2)}) copy-start(f32[2048]{0:T(1024)} %param.16) | copy-start | bytes 24580
  383.1 38.0 %copy-start.16 = (f32[128]{0:T(128)S(1)}, f32[128]{0:T(128)}, u32[]{:S(2)}) copy-start(f32[128]{0:T(128)} %param.25) | copy-start | bytes 1540
  384.1 46.5 %all-to-all-start = ((bf16[128,4,512]{2,0,1:T(8,128)(2,1)}), bf16[128,4,512]{2,0,1:T(8,128)(2,1)S(1)}, u32[]{:S(2)}, u32[]{:S(2)}) async-start(bf16[128,4,512]{2,0,1:T(8,128)(2,1)} %copy.17), calls=%async_computation.1 | async-start | bytes 1048576 | tf_op jit(solution)/shard_map/all_to_all | solution.py:96
  387.6 64.9 %all-gather.17.cloned.1.call-start = ((), (), s32[]{:S(2)}) async-start(), calls=%async_computation.9 | async-start | bytes 1966080 | tf_op jit(solution)/shard_map/all_gather | solution.py:12
  423.2 8.0 %copy-start = (bf16[384,512]{1,0:T(8,128)(2,1)S(1)}, bf16[384,512]{1,0:T(8,128)(2,1)}, u32[]{:S(2)}) copy-start(bf16[384,512]{1,0:T(8,128)(2,1)} %add_convert_fusion.2) | copy-start | bytes 1179652
  423.2 8.0 %copy-start.10 = (f32[512]{0:T(512)S(1)}, f32[512]{0:T(512)}, u32[]{:S(2)}) copy-start(f32[512]{0:T(512)} %param.27) | copy-start | bytes 6148
  431.2 23.0 %copy-start.15 = (f32[2048]{0:T(1024)S(1)}, f32[2048]{0:T(1024)}, u32[]{:S(2)}) copy-start(f32[2048]{0:T(1024)} %param.17) | copy-start | bytes 24580
  432.1 68.8 %reduce-scatter.5.cloned.1.call-start = ((), (), s32[]{:S(2)}) async-start(), calls=%async_computation.10 | async-start | bytes 1966080 | tf_op jit(solution)/shard_map/reduce_scatter | solution.py:19
  454.3 7.3 %copy-start.3 = (bf16[384,2048]{1,0:T(8,128)(2,1)S(1)}, bf16[384,2048]{1,0:T(8,128)(2,1)}, u32[]{:S(2)}) copy-start(bf16[384,2048]{1,0:T(8,128)(2,1)} %all-gather.17.cloned.1.call-done) | copy-start | bytes 4718596
  461.5 39.4 %copy-start.1 = (bf16[384,512]{1,0:T(8,128)(2,1)S(1)}, bf16[384,512]{1,0:T(8,128)(2,1)}, u32[]{:S(2)}) copy-start(bf16[384,512]{1,0:T(8,128)(2,1)} %add_convert_fusion.1) | copy-start | bytes 1179652
Sparse Core Ops, SparseCore 0:
  8.9 22.3 all-gather.6
  33.5 92.2 all-gather.8
  128.0 90.4 all-gather.10
  220.4 91.2 all-gather.12
  323.1 26.1 reduce-scatter.2
  351.4 19.6 all-gather.14
  432.3 20.1 all-gather.16
  472.9 27.9 reduce-scatter.4
where the time goes:
time: 510 us
  waiting for transfers between devices  366 us (72%)
  blocking collectives  69.9 us (14%)
  matrix products  39.5 us (8%)
  other arithmetic  14.9 us (3%)
  between operations  13.8 us (3%)
    all_gather x1, waiting for transfers between devices, body(): lax.all_gather(down_half, 'fs', axis=1, tiled=True)  93.2 us
    all_gather x1, waiting for transfers between devices, body(): lax.all_gather(gate_half, 'fs', axis=0, tiled=True)  92.7 us
    all_gather x1, waiting for transfers between devices, body(): lax.all_gather(up_half, 'fs', axis=0, tiled=True)  85.6 us
    reduce_scatter x2, waiting for transfers between devices, residual_add(): lax.psum_scatter(partial_value.astype(jnp.bfloat16), 'tp', scatter_dimens...  54.4 us
    all_gather x3, waiting for transfers between devices, normed(): gathered = lax.all_gather(own_columns, 'tp', axis=1, tiled=True)  39.1 us
    all_gather x1, blocking collectives, body(): lax.all_gather(out_half, 'fs', axis=1, tiled=True)  31.7 us
    all_gather x1, blocking collectives, body(): lax.all_gather(in_half, 'fs', axis=0, tiled=True)  31.5 us
    dot_general x2, matrix products, feed_forward(): return jnp.dot(hidden, down_whole, preferred_element_type=jnp.float32)  22.5 us
  transfers between devices with their start and end apart: 9, of which 7 were waited for; matrix products, arithmetic and copies ran while one was open for 4% of the time, Pallas kernels for 0%

commit v1 on v0

--- a/solution.py
+++ b/solution.py
@@ -70,7 +70,9 @@
     in_half = pool_in_weight.astype(jnp.bfloat16)
     out_half = pool_out_weight.astype(jnp.bfloat16)
     in_whole, out_whole = (
-        lax.all_gather(in_half, "fs", axis=0, tiled=True),
+        jnp.concatenate(
+            lax.all_to_all(jnp.stack([in_half] * lax.axis_size("fs")), "fs", 0, 0), axis=0
+        ),
         lax.all_gather(out_half, "fs", axis=1, tiled=True),
     )
     gate_whole, up_whole, down_whole = (

time: 510 us -> 490 us (0.961)
  blocking collectives: 69.9 us -> 48.6 us
  starting transfers between devices: 3.94 us -> 9.46 us
    all_gather x1 -> x0, blocking collectives: 31.5 us -> none  [body(): lax.all_gather(in_half, 'fs', axis=0, tiled=True)]
    all_gather x1, blocking collectives: 31.7 us -> 38.3 us  [body(): lax.all_gather(out_half, 'fs', axis=1, tiled=True)]
    all_to_all x0 -> x1, starting transfers between devices: none -> 5.5 us  [body(): lax.all_to_all(jnp.stack([in_half] * lax.axis_size('fs')), 'fs', 0, 0)]
  transfers between devices with their start and end apart: 9 -> 10, of which waited for: 7 -> 7; matrix products, arithmetic and copies ran while one was open for 4% -> 4% of each run, Pallas kernels for 0% -> 0%
where the time goes in v1:
time: 490 us; the launch traced here: 489 us
  waiting for transfers between devices  362 us (74%)
  blocking collectives  48.6 us (10%)
  matrix products  38.1 us (8%)
  other arithmetic  15 us (3%)
  between operations  13.8 us (3%)
  starting transfers between devices  9.46 us (2%)
    all_gather x1, waiting for transfers between devices, body(): lax.all_gather(down_half, 'fs', axis=1, tiled=True)  93.2 us
    all_gather x1, waiting for transfers between devices, body(): lax.all_gather(gate_half, 'fs', axis=0, tiled=True)  92.7 us
    all_gather x1, waiting for transfers between devices, body(): lax.all_gather(up_half, 'fs', axis=0, tiled=True)  85.6 us
    reduce_scatter x2, waiting for transfers between devices, residual_add(): lax.psum_scatter(partial_value.astype(jnp.bfloat16), 'tp', scatter_dimens...  54.5 us
    all_gather x1, blocking collectives, body(): lax.all_gather(out_half, 'fs', axis=1, tiled=True)  38.3 us
    all_gather x3, waiting for transfers between devices, normed(): gathered = lax.all_gather(own_columns, 'tp', axis=1, tiled=True)  34.9 us
    dot_general x2, matrix products, feed_forward(): return jnp.dot(hidden, down_whole, preferred_element_type=jnp.float32)  22.5 us
    dot_general x2, matrix products, feed_forward(): jnp.dot(normed_rows, gate_whole, preferred_element_type=jnp.float32)  14.4 us
  transfers between devices with their start and end apart: 10, of which 7 were waited for; matrix products, arithmetic and copies ran while one was open for 4% of the time, Pallas kernels for 0%

profile of v1, /device:TPU:0, one launch (start us, length us, event | category | flops | bytes accessed | tf_op | source)
XLA Modules:
  0.0 489.4 jit_solution(6346696547886097742)
XLA Ops:
  6.5 0.0 all-gather.7.cloned.1.call-start
  6.5 0.7 all-gather.7.cloned.1.call-update
  7.3 0.0 all-gather.9.cloned.1.call-start
  7.3 2.3 convert_element_type.144
  9.6 0.0 all-gather.9.cloned.1.call-update
  9.7 0.0 all-gather.11.cloned.1.call-start
  9.7 0.0 copy-done.6
  9.7 1.0 convert_element_type.145
  10.7 0.0 all-gather.11.cloned.1.call-update
  10.7 0.0 copy-start.12
  10.7 0.0 copy-start.14
  10.7 0.0 all-gather.13.cloned.1.call-start
  10.8 0.5 copy-done.7
  11.3 1.0 convert_element_type.147
  12.2 0.0 all-gather.13.cloned.1.call-update
  12.2 0.0 reduce-scatter.3.cloned.1.call-start
  12.3 19.0 %all-gather.7.cloned.1.call-done = bf16[384,2048]{1,0:T(8,128)(2,1)} async-done(((bf16[384,512]{1,0:T(8,128)(2,1)}), bf16[384,2048]{1,0:T(8,128)(2,1)}) %all-gather.7.cloned.1.call-update) | async-done | bytes 1572880 | tf_op jit(solution)/shard_map/all_gather | solution.py:12
  31.3 1.8 fusion
  33.1 0.0 copy-start.15
  33.1 92.7 %all-gather.9.cloned.1.call-done = bf16[2048,1408]{1,0:T(8,128)(2,1)} async-done(((bf16[256,1408]{1,0:T(8,128)(2,1)}), bf16[2048,1408]{1,0:T(8,128)(2,1)}) %all-gather.9.cloned.1.call-update) | async-done | bytes 5767184 | tf_op jit(solution)/shard_map/all_gather | solution.py:79
  125.8 7.1 %convolution_multiply_fusion.3 = f32[384,1408]{1,0:T(8,128)} fusion(bf16[2048,1408]{1,0:T(8,128)(2,1)} %all-gather.9.cloned.1.call-done, f32[1408]{0:T(1024)S(1)} %copy-done.14, bf16[384,2048]{1,0:T(8,128)(2,1)} %all-gather.7.cloned.1.call-done, f32[2048]{0:T(1024)S(1)} %copy-done.12, f32[384]{0:T(512)S(1)} %add_rsqrt_fusion.2), kind=kOutput, calls=%fused_computation.21 | convolution fusion | flops 2218278912 | bytes 9518080 | tf_op jit(solution)/shard_map/dot_general | solution.py:85
  132.9 85.6 %all-gather.11.cloned.1.call-done = bf16[2048,1408]{1,0:T(8,128)(2,1)} async-done(((bf16[256,1408]{1,0:T(8,128)(2,1)}), bf16[2048,1408]{1,0:T(8,128)(2,1)}) %all-gather.11.cloned.1.call-update) | async-done | bytes 5767184 | tf_op jit(solution)/shard_map/all_gather | solution.py:80
  218.5 93.2 %all-gather.13.cloned.1.call-done = bf16[1408,2048]{1,0:T(8,128)(2,1)} async-done(((bf16[1408,256]{1,0:T(8,128)(2,1)}), bf16[1408,2048]{1,0:T(8,128)(2,1)}) %all-gather.13.cloned.1.call-update) | async-done | bytes 5767184 | tf_op jit(solution)/shard_map/all_gather | solution.py:81
  311.8 0.0 copy-done.3
  311.8 11.2 %convolution_convert_fusion.1 = bf16[384,2048]{1,0:T(8,128)(2,1)} fusion(bf16[1408,2048]{1,0:T(8,128)(2,1)} %all-gather.13.cloned.1.call-done, bf16[2048,1408]{1,0:T(8,128)(2,1)} %all-gather.11.cloned.1.call-done, f32[384,1408]{1,0:T(8,128)} %convolution_multiply_fusion.3, f32[1408]{0:T(1024)S(1)} %copy-done.15, bf16[384,2048]{1,0:T(8,128)(2,1)S(1)} %copy-done.3, ...), kind=kOutput, calls=%fused_computation.23 | convolution fusion | flops 4436901888 | bytes 16858112 | tf_op jit(solution)/shard_map/dot_general | solution.py:88
  323.0 0.0 reduce-scatter.3.cloned.1.call-update
  323.0 0.0 all-gather.15.cloned.1.call-start
  323.1 26.3 %reduce-scatter.3.cloned.1.call-done = bf16[384,512]{1,0:T(8,128)(2,1)} async-done(((bf16[384,2048]{1,0:T(8,128)(2,1)}), bf16[384,512]{1,0:T(8,128)(2,1)}) %reduce-scatter.3.cloned.1.call-update) | async-done | bytes 393232 | tf_op jit(solution)/shard_map/reduce_scatter | solution.py:19
  349.4 0.0 copy-done.10
  349.4 1.9 add_convert_fusion.2
  351.3 0.0 all-gather.15.cloned.1.call-update
  351.4 0.9 stack.2
  352.2 5.5 %all-to-all-start = ((bf16[8,256,128]{2,1,0:T(8,128)(2,1)}), bf16[8,256,128]{2,1,0:T(8,128)(2,1)S(1)}, u32[]{:S(2)}, u32[]{:S(2)}) async-start(bf16[8,256,128]{2,1,0:T(8,128)(2,1)} %stack.2), calls=%async_computation.1 | async-start | bytes 1048576 | tf_op jit(solution)/shard_map/all_to_all | solution.py:74
  357.7 0.1 copy.16
  357.8 0.0 copy-start.13
  357.9 0.0 copy-start.17
  357.9 38.3 %all_gather.30 = bf16[128,2048]{0,1:T(8,128)(2,1)S(1)} all-gather(bf16[128,256]{0,1:T(8,128)(2,1)S(1)} %copy.16), channel_id=1, replica_groups=mesh['fs'=8,'tp'=4] {'fs'}, dimensions={1}, use_global_device_ids=true | all-gather | bytes 589824 | tf_op jit(solution)/shard_map/all_gather | solution.py:76
  396.2 1.0 copy.17
  397.3 0.0 all-gather.15.cloned.1.call-done
  397.3 1.9 fusion.3
  399.2 0.0 all-to-all-done
  399.3 3.5 all-to-all-start.1
  402.7 0.0 all-gather.17.cloned.1.call-start
  402.8 0.6 fusion.20
  403.5 0.0 copy-start
  403.5 0.0 copy-start.11
  403.5 0.2 reduce_window_sum.11
  403.8 0.3 fusion.46
  404.1 0.1 copy.15
  404.2 10.3 %all_gather.29 = bf16[384,512]{0,1:T(8,128)(2,1)S(1)} all-gather(bf16[384,128]{0,1:T(8,128)(2,1)S(1)} %copy.15), channel_id=1, replica_groups=mesh['fs'=8,'tp'=4] {'tp'}, dimensions={1}, use_global_device_ids=true | all-gather | bytes 491520 | tf_op jit(solution)/shard_map/all_gather | solution.py:97
  414.5 0.0 all-to-all-done.1
  414.5 0.6 convert_reduce_fusion
  415.1 0.0 copy-start.16
  415.1 0.9 add_convert_fusion.1
  416.0 0.0 all-gather.17.cloned.1.call-update
  416.0 0.2 reduce-scatter.5.cloned.1.call-start
  416.3 15.9 %all-gather.17.cloned.1.call-done = bf16[384,2048]{1,0:T(8,128)(2,1)} async-done(((bf16[384,512]{1,0:T(8,128)(2,1)}), bf16[384,2048]{1,0:T(8,128)(2,1)}) %all-gather.17.cloned.1.call-update) | async-done | bytes 1572880 | tf_op jit(solution)/shard_map/all_gather | solution.py:12
  432.2 1.8 fusion.6
  434.0 7.2 %convolution_multiply_fusion.1 = f32[384,1408]{1,0:T(8,128)} fusion(bf16[2048,1408]{1,0:T(8,128)(2,1)} %all-gather.9.cloned.1.call-done, f32[1408]{0:T(1024)S(1)} %copy-done.14, bf16[384,2048]{1,0:T(8,128)(2,1)} %all-gather.17.cloned.1.call-done, f32[2048]{0:T(1024)S(1)} %copy-done.16, f32[384]{0:T(512)S(1)} %add_rsqrt_fusion), kind=kOutput, calls=%fused_computation.18 | convolution fusion | flops 2218278912 | bytes 9518080 | tf_op jit(solution)/shard_map/dot_general | solution.py:85
  441.2 0.0 copy-done.4
  441.2 11.3 %convolution_convert_fusion = bf16[384,2048]{1,0:T(8,128)(2,1)} fusion(bf16[1408,2048]{1,0:T(8,128)(2,1)} %all-gather.13.cloned.1.call-done, bf16[2048,1408]{1,0:T(8,128)(2,1)} %all-gather.11.cloned.1.call-done, f32[384,1408]{1,0:T(8,128)} %convolution_multiply_fusion.1, f32[1408]{0:T(1024)S(1)} %copy-done.15, bf16[384,2048]{1,0:T(8,128)(2,1)S(1)} %copy-done.4, ...), kind=kOutput, calls=%fused_computation.22 | convolution fusion | flops 4436901888 | bytes 16858112 | tf_op jit(solution)/shard_map/dot_general | solution.py:88
  452.5 0.0 reduce-scatter.5.cloned.1.call-update
  452.5 28.2 %reduce-scatter.5.cloned.1.call-done = bf16[384,512]{1,0:T(8,128)(2,1)} async-done(((bf16[384,2048]{1,0:T(8,128)(2,1)}), bf16[384,512]{1,0:T(8,128)(2,1)}) %reduce-scatter.5.cloned.1.call-update) | async-done | bytes 393232 | tf_op jit(solution)/shard_map/reduce_scatter | solution.py:19
  480.7 1.9 add_convert_fusion
  (42 shorter events, 0.2 us)
Async XLA Ops:
  6.5 3.2 copy-start.6
  6.5 24.7 %all-gather.7.cloned.1.call-start = ((), (), s32[]{:S(2)}) async-start(), calls=%async_computation.4 | async-start | bytes 1966080 | tf_op jit(solution)/shard_map/all_gather | solution.py:12
  7.3 118.5 %all-gather.9.cloned.1.call-start = ((), (), s32[]{:S(2)}) async-start(), calls=%async_computation.5 | async-start | bytes 6488064 | tf_op jit(solution)/shard_map/all_gather | solution.py:79
  9.6 1.6 copy-start.7
  9.7 208.9 %all-gather.11.cloned.1.call-start = ((), (), s32[]{:S(2)}) async-start(), calls=%async_computation.6 | async-start | bytes 6488064 | tf_op jit(solution)/shard_map/all_gather | solution.py:80
  10.7 115.1 %copy-start.12 = (f32[2048]{0:T(1024)S(1)}, f32[2048]{0:T(1024)}, u32[]{:S(2)}) copy-start(f32[2048]{0:T(1024)} %param.15) | copy-start | bytes 24580
  10.7 115.1 %copy-start.14 = (f32[1408]{0:T(1024)S(1)}, f32[1408]{0:T(1024)}, u32[]{:S(2)}) copy-start(f32[1408]{0:T(1024)} %param.19) | copy-start | bytes 16900
  10.7 301.0 %all-gather.13.cloned.1.call-start = ((), (), s32[]{:S(2)}) async-start(), calls=%async_computation.7 | async-start | bytes 6488064 | tf_op jit(solution)/shard_map/all_gather | solution.py:81
  12.2 337.2 %reduce-scatter.3.cloned.1.call-start = ((), (), s32[]{:S(2)}) async-start(), calls=%async_computation.8 | async-start | bytes 1966080 | tf_op jit(solution)/shard_map/reduce_scatter | solution.py:19
  33.1 278.7 %copy-start.3 = (bf16[384,2048]{1,0:T(8,128)(2,1)S(1)}, bf16[384,2048]{1,0:T(8,128)(2,1)}, u32[]{:S(2)}) copy-start(bf16[384,2048]{1,0:T(8,128)(2,1)} %all-gather.7.cloned.1.call-done) | copy-start | bytes 4718596
  33.1 278.7 %copy-start.15 = (f32[1408]{0:T(1024)S(1)}, f32[1408]{0:T(1024)}, u32[]{:S(2)}) copy-start(f32[1408]{0:T(1024)} %param.21) | copy-start | bytes 16900
  132.9 216.5 %copy-start.5 = (bf16[384,512]{1,0:T(8,128)(2,1)S(1)}, bf16[384,512]{1,0:T(8,128)(2,1)}, u32[]{:S(2)}) copy-start(bf16[384,512]{1,0:T(8,128)(2,1)} %param.14) | copy-start | bytes 1179652
  132.9 216.5 %copy-start.10 = (f32[512]{0:T(512)S(1)}, f32[512]{0:T(512)}, u32[]{:S(2)}) copy-start(f32[512]{0:T(512)} %param.23) | copy-start | bytes 6148
  323.0 28.3 %copy-start.8 = (f32[256,128]{1,0:T(8,128)S(1)}, f32[256,128]{1,0:T(8,128)}, u32[]{:S(2)}) copy-start(f32[256,128]{1,0:T(8,128)} %param.24) | copy-start | bytes 393220
  323.0 34.7 %copy-start.9 = (f32[128,256]{1,0:T(8,128)S(1)}, f32[128,256]{1,0:T(8,128)}, u32[]{:S(2)}) copy-start(f32[128,256]{1,0:T(8,128)} %param.26) | copy-start | bytes 393220
  323.0 74.3 %all-gather.15.cloned.1.call-start = ((), (), s32[]{:S(2)}) async-start(), calls=%async_computation.9 | async-start | bytes 1966080 | tf_op jit(solution)/shard_map/all_gather | solution.py:12
  352.2 47.0 %all-to-all-start = ((bf16[8,256,128]{2,1,0:T(8,128)(2,1)}), bf16[8,256,128]{2,1,0:T(8,128)(2,1)S(1)}, u32[]{:S(2)}, u32[]{:S(2)}) async-start(bf16[8,256,128]{2,1,0:T(8,128)(2,1)} %stack.2), calls=%async_computation.1 | async-start | bytes 1048576 | tf_op jit(solution)/shard_map/all_to_all | solution.py:74
  357.8 44.9 %copy-start.13 = (f32[2048]{0:T(1024)S(1)}, f32[2048]{0:T(1024)}, u32[]{:S(2)}) copy-start(f32[2048]{0:T(1024)} %param.16) | copy-start | bytes 24580
  357.9 44.9 %copy-start.17 = (f32[128]{0:T(128)S(1)}, f32[128]{0:T(128)}, u32[]{:S(2)}) copy-start(f32[128]{0:T(128)} %param.25) | copy-start | bytes 1540
  397.3 5.5 %copy-start.2 = (bf16[384,2048]{1,0:T(8,128)(2,1)S(1)}, bf16[384,2048]{1,0:T(8,128)(2,1)}, u32[]{:S(2)}) copy-start(bf16[384,2048]{1,0:T(8,128)(2,1)} %all-gather.15.cloned.1.call-done) | copy-start | bytes 4718596
  399.3 15.2 %all-to-all-start.1 = ((bf16[128,4,512]{2,0,1:T(8,128)(2,1)}), bf16[128,4,512]{2,0,1:T(8,128)(2,1)S(1)}, u32[]{:S(2)}, u32[]{:S(2)}) async-start(bf16[128,4,512]{2,0,1:T(8,128)(2,1)} %copy.17), calls=%async_computation.2 | async-start | bytes 1048576 | tf_op jit(solution)/shard_map/all_to_all | solution.py:98
  402.7 29.4 %all-gather.17.cloned.1.call-start = ((), (), s32[]{:S(2)}) async-start(), calls=%async_computation.10 | async-start | bytes 1966080 | tf_op jit(solution)/shard_map/all_gather | solution.py:12
  403.5 11.6 %copy-start = (bf16[384,512]{1,0:T(8,128)(2,1)S(1)}, bf16[384,512]{1,0:T(8,128)(2,1)}, u32[]{:S(2)}) copy-start(bf16[384,512]{1,0:T(8,128)(2,1)} %add_convert_fusion.2) | copy-start | bytes 1179652
  403.5 11.6 %copy-start.11 = (f32[512]{0:T(512)S(1)}, f32[512]{0:T(512)}, u32[]{:S(2)}) copy-start(f32[512]{0:T(512)} %param.27) | copy-start | bytes 6148
  415.1 18.8 %copy-start.16 = (f32[2048]{0:T(1024)S(1)}, f32[2048]{0:T(1024)}, u32[]{:S(2)}) copy-start(f32[2048]{0:T(1024)} %param.17) | copy-start | bytes 24580
  416.0 64.6 %reduce-scatter.5.cloned.1.call-start = ((), (), s32[]{:S(2)}) async-start(), calls=%async_computation.11 | async-start | bytes 1966080 | tf_op jit(solution)/shard_map/reduce_scatter | solution.py:19
  434.0 7.2 %copy-start.4 = (bf16[384,2048]{1,0:T(8,128)(2,1)S(1)}, bf16[384,2048]{1,0:T(8,128)(2,1)}, u32[]{:S(2)}) copy-start(bf16[384,2048]{1,0:T(8,128)(2,1)} %all-gather.17.cloned.1.call-done) | copy-start | bytes 4718596
  441.2 39.5 %copy-start.1 = (bf16[384,512]{1,0:T(8,128)(2,1)S(1)}, bf16[384,512]{1,0:T(8,128)(2,1)}, u32[]{:S(2)}) copy-start(bf16[384,512]{1,0:T(8,128)(2,1)} %add_convert_fusion.1) | copy-start | bytes 1179652
Sparse Core Ops, SparseCore 0:
  8.9 22.3 all-gather.6
  33.5 92.2 all-gather.8
  128.0 90.4 all-gather.10
  220.4 91.2 all-gather.12
  323.2 26.2 reduce-scatter.2
  351.5 19.6 all-gather.14
  416.2 15.9 all-gather.16
  452.6 28.0 reduce-scatter.4
